TPU v7x, 32 devices: a whole 2x2x4 slice. The times are simulated.
32 devices in a mesh: fs: 16 (over z, y, x), tp: 2 (over core).
Axes of the slice: x: 2, y: 2, z: 4, core: 2. Of those that a mesh axis runs over, the one named last changes fastest.
Arguments:
- tokens: bfloat16 [12288, 2048], P('fs'), may hold values from -6 to 6
- norm_gain: float32 [2048], replicated, may hold values from 0.1 to 1.9
- gate_weight: bfloat16 [2048, 5120], P('fs', 'tp'), may hold values from -0.125 to 0.125
- up_weight: bfloat16 [2048, 5120], P('fs', 'tp'), may hold values from -0.125 to 0.125
- down_weight: bfloat16 [5120, 2048], P('tp', 'fs'), may hold values from -0.078125 to 0.078125
Outputs:
- mixed: bfloat16 [12288, 2048], P(('fs', 'tp'))
All inputs are finite; a program needn't handle non-finite values.
Results may differ from a plain program's by a relative error of at most 0.014.
Values may be sent and summed in bfloat16 or wider, within the bound.
A program may use at most 128 MiB of HBM per device.

v0:
```python
import functools

import jax
import jax.numpy as jnp
from jax import lax
from jax.experimental import pallas as pl
from jax.experimental.pallas import tpu as pltpu
from jax.sharding import PartitionSpec as P

MESH = pl.DeviceIdType.MESH
PLANE = 4
ORDER = ((1, 1), (0, 1), (1, 0), (0, 0))


def simple(tokens, norm_gain, gate_weight, up_weight, down_weight):
    values = tokens.astype(jnp.float32)
    scale = lax.rsqrt(jnp.mean(values * values, axis=-1, keepdims=True) + 1e-06)
    normed = (values * scale * norm_gain).astype(jnp.bfloat16)

    def project(piece):
        whole = lax.all_gather(piece, "fs", axis=0, tiled=True)
        return jnp.dot(normed, whole, preferred_element_type=jnp.float32)

    hidden = (jax.nn.silu(project(gate_weight)) * project(up_weight)).astype(jnp.bfloat16)
    down_whole = lax.all_gather(down_weight, "fs", axis=1, tiled=True)
    return lax.psum_scatter(
        jnp.dot(hidden, down_whole, preferred_element_type=jnp.float32).astype(jnp.bfloat16),
        "tp",
        scatter_dimension=0,
        tiled=True,
    )


def kernel(nz, tok_hbm, gain_ref, gate_hbm, up_hbm, down_hbm, out_ref,
           tok, acc, gu, dn, hidden, psend, precv, own,
           loc_sem, a2a_s, a2a_r, tok_s, tok_r, up_s, dn_s, z_r, sib_s, sib_r, one_s, one_r, rs_s, rs_r):
    f = lax.axis_index("fs")
    c = lax.axis_index("tp")
    z, p = f // PLANE, f % PLANE
    y, x = p // 2, p % 2
    depth = gate_hbm.shape[0]
    width = gate_hbm.shape[1] // PLANE
    rows = tok_hbm.shape[0] // 2
    unit = depth * PLANE

    def member(k):
        oy, ox = ORDER[k]
        return ((y + oy) % 2) * 2 + (x + ox) % 2

    def dev(plane, z_, core):
        return (z_ * PLANE + plane, core)

    barrier = pltpu.get_barrier_semaphore()
    for k in range(3):
        pl.semaphore_signal(barrier, inc=1, device_id=dev(member(k), z, c), device_id_type=MESH)
    pl.semaphore_signal(barrier, inc=1, device_id=(f, 1 - c), device_id_type=MESH)

    @pl.when(z > 0)
    def _():
        pl.semaphore_signal(barrier, inc=1, device_id=dev(p, z - 1, c), device_id_type=MESH)

    @pl.when(z < nz - 1)
    def _():
        pl.semaphore_signal(barrier, inc=1, device_id=dev(p, z + 1, c), device_id_type=MESH)

    pl.semaphore_wait(barrier, 4 + (z + nz - 1) // nz + (2 * nz - 2 - z) // nz)

    sources = (gate_hbm, up_hbm, down_hbm)

    def piece_src(m, q):
        start = pl.multiple_of(q * width, 128)
        if m < 2:
            return sources[m].at[:, pl.ds(start, width)]
        return sources[m].at[pl.ds(start, width), :]

    def weight_dst(m, start, size):
        start = pl.multiple_of(start, 128)
        units = pl.ds(pl.multiple_of(c * width, 128), width)
        if m < 2:
            return gu.at[m, pl.ds(start, size), units]
        return dn.at[units, pl.ds(start, size)]

    def weight_sib(m, start, size):
        start = pl.multiple_of(start, 128)
        units = pl.ds(pl.multiple_of((1 - c) * width, 128), width)
        if m < 2:
            return gu.at[m, pl.ds(start, size), units]
        return dn.at[units, pl.ds(start, size)]

    def a2a(m, k):
        q = member(k)
        return pltpu.make_async_remote_copy(
            src_ref=piece_src(m, q), dst_ref=weight_dst(m, f * depth, depth),
            send_sem=a2a_s.at[m, k], recv_sem=a2a_r.at[m, k],
            device_id=dev(q, z, c), device_id_type=MESH)

    def a2a_in(m, k):
        q = member(k)
        ref = weight_dst(m, (z * PLANE + q) * depth, depth)
        return pltpu.make_async_remote_copy(
            src_ref=ref, dst_ref=ref, send_sem=a2a_s.at[m, k], recv_sem=a2a_r.at[m, k],
            device_id=dev(q, z, c), device_id_type=MESH)

    def local(m):
        return pltpu.make_async_copy(piece_src(m, p), weight_dst(m, f * depth, depth), loc_sem.at[m])

    half = pl.ds(pl.multiple_of(c * rows, 16), rows)

    def tok_copy(k):
        q = member(k)
        return pltpu.make_async_remote_copy(
            src_ref=tok_hbm.at[half, :], dst_ref=tok.at[k],
            send_sem=tok_s.at[k], recv_sem=tok_r.at[k],
            device_id=dev(q, z, c), device_id_type=MESH)

    own_tok = pltpu.make_async_copy(tok_hbm.at[half, :], tok.at[3], loc_sem.at[3])

    def along(m, zs, step):
        ref = weight_dst(m, zs * unit, unit)
        sems = up_s if step > 0 else dn_s
        return pltpu.make_async_remote_copy(
            src_ref=ref, dst_ref=ref, send_sem=sems.at[m, zs], recv_sem=z_r.at[m, zs],
            device_id=dev(p, z + step, c), device_id_type=MESH)

    def to_sibling(m, zs):
        ref = weight_dst(m, zs * unit, unit)
        return pltpu.make_async_remote_copy(
            src_ref=ref, dst_ref=ref, send_sem=sib_s.at[m, zs], recv_sem=sib_r.at[m, zs],
            device_id=(f, 1 - c), device_id_type=MESH)

    def from_sibling(m, zs):
        ref = weight_sib(m, zs * unit, unit)
        return pltpu.make_async_remote_copy(
            src_ref=ref, dst_ref=ref, send_sem=sib_s.at[m, zs], recv_sem=sib_r.at[m, zs],
            device_id=(f, 1 - c), device_id_type=MESH)

    def forward(m, zs):
        @pl.when((zs <= z) & (z < nz - 1))
        def _():
            along(m, zs, 1).start()

        @pl.when((zs >= z) & (z > 0))
        def _():
            along(m, zs, -1).start()

        to_sibling(m, zs).start()

    def arrived(m, zs):
        along(m, zs, 1).wait_recv()

    def piece(m, k, step):
        ref = weight_dst(m, (z * PLANE + member(k)) * depth, depth)
        sems = up_s if step > 0 else dn_s
        return pltpu.make_async_remote_copy(
            src_ref=piece_src(m, p) if k == 3 else ref, dst_ref=ref,
            send_sem=sems.at[m, z], recv_sem=z_r.at[m, z],
            device_id=dev(p, z + step, c), device_id_type=MESH)

    def pass_piece(m, k):
        @pl.when(z < nz - 1)
        def _():
            piece(m, k, 1).start()

        @pl.when(z > 0)
        def _():
            piece(m, k, -1).start()

    for m in range(3):
        for k in (1, 2, 0):
            a2a(m, k).start()
        local(m).start()
        if m < 2:
            pass_piece(m, 3)
    for k in (1, 2, 0):
        tok_copy(k).start()
    own_tok.start()

    def own_unit(m):
        if m == 2:
            pass_piece(m, 3)
        for k in (1, 2, 0):
            a2a_in(m, k).wait_recv()
            pass_piece(m, k)
        local(m).wait()
        to_sibling(m, z).start()

    own_unit(0)
    own_unit(1)
    def relay_wide(d):
        for m in range(2):
            @pl.when(z - d >= 0)
            def _():
                arrived(m, z - d)
                forward(m, z - d)

            @pl.when(z + d < nz)
            def _():
                arrived(m, z + d)
                forward(m, z + d)
    for d in range(1, nz - 1):
        relay_wide(d)
    own_unit(2)
    inner = (z > 0) & (z < nz - 1)

    def relay_down(d):
        @pl.when(inner & (z - d >= 0))
        def _():
            arrived(2, z - d)
            forward(2, z - d)

        @pl.when(inner & (z + d < nz))
        def _():
            arrived(2, z + d)
            forward(2, z + d)

    end = z // (nz - 1)
    late = (nz - 1) * (1 - end)

    def project(m, k, at, start, size):
        depths = pl.ds(pl.multiple_of(start * unit, 128), size * unit)
        return jnp.dot(tok[k, :, depths], gu[m, depths, at], preferred_element_type=jnp.float32)

    for m in range(2):
        for i in range(nz - 1):
            from_sibling(m, end + i).wait_recv()
    for k in (3, 1, 2, 0):
        if k == 3:
            own_tok.wait()
        else:
            tok_copy(k).wait_recv()
        block = rows // 6

        @pl.loop(0, 6)
        def _(i):
            at = pl.ds(pl.multiple_of(i * block, 16), block)
            values = tok[k, at, :].astype(jnp.float32)
            scale = lax.rsqrt(jnp.mean(values * values, axis=-1, keepdims=True) + 1e-06)
            tok[k, at, :] = (values * scale * gain_ref[...]).astype(jnp.bfloat16)

        @pl.loop(0, 2 * width // 256)
        def _(j):
            at = pl.ds(pl.multiple_of(j * 256, 256), 256)
            for m in range(2):
                acc[m, k, :, at] = project(m, k, at, end, nz - 1)

    relay_wide(nz - 1)
    for m in range(2):
        from_sibling(m, late).wait_recv()

    def make_hidden(k):
        @pl.loop(0, 2 * width // 256)
        def _(j):
            at = pl.ds(pl.multiple_of(j * 256, 256), 256)
            gate = acc[0, k, :, at] + project(0, k, at, late, 1)
            up = acc[1, k, :, at] + project(1, k, at, late, 1)
            hidden[k, :, at] = (gate / (1.0 + jnp.exp(-gate)) * up).astype(jnp.bfloat16)

    part_rows = (pl.ds(0, rows // 2), pl.ds(rows // 2, rows // 2))

    def first(h, step):
        at = (0, part_rows[h], columns_at(step))
        return pltpu.make_async_remote_copy(
            src_ref=psend.at[at], dst_ref=precv.at[at],
            send_sem=one_s.at[h, step], recv_sem=one_r.at[h, step],
            device_id=dev(member(1 + h), z, c), device_id_type=MESH)

    def last(k, h, step):
        at = (k, part_rows[h], columns_at(step))
        return pltpu.make_async_remote_copy(
            src_ref=psend.at[at], dst_ref=precv.at[at],
            send_sem=rs_s.at[2 * k + h - 2, step], recv_sem=rs_r.at[2 * k + h - 2, step],
            device_id=dev(member(k), z, c), device_id_type=MESH)

    def plane_at(step):
        return (z + step * (1 - 2 * (z // (nz // 2))) + nz) % nz

    def columns_at(step):
        return pl.ds(pl.multiple_of(plane_at(step) * unit, 128), unit)

    def add_and_send(step):
        for h in range(2):
            k = 2 - h
            first(h, step).wait_recv()
            at = (part_rows[h], columns_at(step))
            psend[(k, *at)] = (
                psend[(k, *at)].astype(jnp.float32) + precv[(0, *at)].astype(jnp.float32)
            ).astype(jnp.bfloat16)
            last(k, h, step).start()

    for step in range(nz):
        zs = plane_at(step)
        if step > 0:
            @pl.when(jnp.logical_not(inner))
            def _():
                arrived(2, zs)
                to_sibling(2, zs).start()

            relay_down(step)
        from_sibling(2, zs).wait_recv()
        for k in range(PLANE):
            if step == 0:
                make_hidden(k)

            @pl.loop(0, unit // 256)
            def _(j):
                at = pl.ds(pl.multiple_of(zs * unit + j * 256, 256), 256)
                part = jnp.dot(hidden[k], dn[:, at], preferred_element_type=jnp.float32)
                if k == 3:
                    own[:, at] = part
                else:
                    psend[k, :, at] = part.astype(jnp.bfloat16)

            if k == 0:
                first(0, step).start()
                first(1, step).start()
            elif k < 3:
                last(k, k - 1, step).start()
        if step == 0:
            add_and_send(0)
        elif step > 1:
            add_and_send(step - 1)
    add_and_send(nz - 1)

    for step in range(nz):
        for k in (1, 2):
            for h in range(2):
                last(k, h, step).wait_recv()

        @pl.loop(0, unit // 256)
        def _(j):
            at = pl.ds(pl.multiple_of(plane_at(step) * unit + j * 256, 256), 256)
            total = own[:, at]
            for k in (1, 2):
                total = total + precv[k, :, at].astype(jnp.float32)
            out_ref[:, at] = total.astype(out_ref.dtype)

    for m in range(3):
        for k in range(3):
            a2a(m, k).wait_send()
        for zs in range(nz):
            to_sibling(m, zs).wait_send()

            @pl.when((zs <= z) & (z < nz - 1))
            def _():
                along(m, zs, 1).wait_send()

            @pl.when((zs >= z) & (z > 0))
            def _():
                along(m, zs, -1).wait_send()
    for k in range(3):
        tok_copy(k).wait_send()
    for step in range(nz):
        for h in range(2):
            first(h, step).wait_send()
            for k in (1, 2):
                last(k, h, step).wait_send()


def fused(nfs, tokens, norm_gain, gate_weight, up_weight, down_weight):
    nz = nfs // PLANE
    features = tokens.shape[1]
    rows = tokens.shape[0] // 2
    width = gate_weight.shape[1] // PLANE
    any_spec = pl.BlockSpec(memory_space=pl.ANY)
    vmem_spec = pl.BlockSpec(memory_space=pltpu.VMEM)
    dma = pltpu.SemaphoreType.DMA
    bf16 = jnp.bfloat16
    return pl.pallas_call(
        functools.partial(kernel, nz),
        out_shape=jax.ShapeDtypeStruct((rows, features), bf16),
        in_specs=[any_spec, vmem_spec, any_spec, any_spec, any_spec],
        out_specs=vmem_spec,
        scratch_shapes=[
            pltpu.VMEM((PLANE, rows, features), bf16),
            pltpu.VMEM((2, PLANE, rows, 2 * width), jnp.float32),
            pltpu.VMEM((2, features, 2 * width), bf16),
            pltpu.VMEM((2 * width, features), bf16),
            pltpu.VMEM((PLANE, rows, 2 * width), bf16),
            pltpu.VMEM((3, rows, features), bf16),
            pltpu.VMEM((3, rows, features), bf16),
            pltpu.VMEM((rows, features), jnp.float32),
            dma((4,)), dma((3, 3)), dma((3, 3)), dma((3,)), dma((3,)),
            dma((3, nz)), dma((3, nz)), dma((3, nz)), dma((3, nz)), dma((3, nz)),
            dma((2, nz)), dma((2, nz)), dma((4, nz)), dma((4, nz)),
        ],
        compiler_params=pltpu.CompilerParams(
            collective_id=0, has_side_effects=True, vmem_limit_bytes=62 * 1024 * 1024
        ),
    )(tokens, norm_gain.reshape(1, features), gate_weight, up_weight, down_weight)


def per_device(nfs, ntp, tokens, norm_gain, gate_weight, up_weight, down_weight):
    rows, depth = tokens.shape[0] // 2, gate_weight.shape[0]
    fits = (
        ntp == 2
        and nfs % PLANE == 0
        and (nfs // PLANE) % 2 == 0
        and rows % 96 == 0
        and depth % 128 == 0
        and depth * nfs == tokens.shape[1]
        and gate_weight.shape[1] % (PLANE * 128) == 0
    )
    body = functools.partial(fused, nfs) if fits else simple
    return body(tokens, norm_gain, gate_weight, up_weight, down_weight)


def solution(mesh):
    in_specs = (P("fs", None), P(), P("fs", "tp"), P("fs", "tp"), P("tp", "fs"))
    out_specs = P(("fs", "tp"), None)
    body = functools.partial(per_device, mesh.shape["fs"], mesh.shape["tp"])
    return jax.shard_map(
        body, mesh=mesh, in_specs=in_specs, out_specs=out_specs, check_vma=False
    )
```

profile of v0, /device:TPU:0, one launch (start us, length us, event | category | flops | bytes accessed | tf_op | source)
XLA Modules:
  0.0 166.4 jit_solution(2477939148938982099)
XLA Ops:
  0.0 163.6 %shard_map.55 = bf16[384,2048]{1,0:T(8,128)(2,1)} custom-call(bf16[768,2048]{1,0:T(8,128)(2,1)} %tok_hbm.1, f32[1,2048]{1,0:T(1,128)} %bitcast.1, bf16[128,2560]{1,0:T(8,128)(2,1)} %gate_hbm.1, bf16[128,2560]{1,0:T(8,128)(2,1)} %up_hbm.1, bf16[2560,128]{1,0:T(8,128)(2,1)} %down_hbm.1), custom_call_target="tpu_custom_call" | custom-call | tf_op jit(solution)/shard_map/pallas_call | solution.py:368
  163.6 2.7 %copy.7 = bf16[384,2048]{1,0:T(8,128)(2,1)} copy(bf16[384,2048]{1,0:T(8,128)(2,1)} %shard_map.55) | data formatting | bytes 3145728
where the time goes:
time: 167 us; the launch traced here: 166 us
  Pallas kernels  164 us (98%)
  local copies, waits for them, and re-layouts  2.73 us (2%)
    pallas_call x1, Pallas kernels, fused(): pl.pallas_call(functools.partial(kernel, nz), out_shape=jax.ShapeDtypeStr...  164 us

commit v1 on v0

--- a/solution.py
+++ b/solution.py
@@ -105,13 +105,18 @@
         return pltpu.make_async_copy(piece_src(m, p), weight_dst(m, f * depth, depth), loc_sem.at[m])
 
     half = pl.ds(pl.multiple_of(c * rows, 16), rows)
-
-    def tok_copy(k):
-        q = member(k)
-        return pltpu.make_async_remote_copy(
-            src_ref=tok_hbm.at[half, :], dst_ref=tok.at[k],
-            send_sem=tok_s.at[k], recv_sem=tok_r.at[k],
-            device_id=dev(q, z, c), device_id_type=MESH)
+    part_rows = (pl.ds(0, rows // 2), pl.ds(rows // 2, rows // 2))
+
+    def tok_part(k, h):
+        ref = psend.at[k, part_rows[h], :]
+        if k == 0:
+            source, to = psend.at[1 + h, part_rows[h], :], member(2 - h)
+        else:
+            start = pl.multiple_of(c * rows + h * (rows // 2), 16)
+            source, to = tok_hbm.at[pl.ds(start, rows // 2), :], member(k)
+        return pltpu.make_async_remote_copy(
+            src_ref=source, dst_ref=ref, send_sem=tok_s.at[k, h], recv_sem=tok_r.at[k, h],
+            device_id=dev(to, z, c), device_id_type=MESH)
 
     own_tok = pltpu.make_async_copy(tok_hbm.at[half, :], tok.at[3], loc_sem.at[3])
 
@@ -165,14 +170,14 @@
         def _():
             piece(m, k, -1).start()
 
-    for m in range(3):
+    for m in range(2):
         for k in (1, 2, 0):
             a2a(m, k).start()
         local(m).start()
-        if m < 2:
-            pass_piece(m, 3)
-    for k in (1, 2, 0):
-        tok_copy(k).start()
+        pass_piece(m, 3)
+    for h in range(2):
+        tok_part(1, h).start()
+        tok_part(2, 1 - h).start()
     own_tok.start()
 
     def own_unit(m):
@@ -186,76 +191,96 @@
 
     own_unit(0)
     own_unit(1)
-    def relay_wide(d):
-        for m in range(2):
-            @pl.when(z - d >= 0)
-            def _():
-                arrived(m, z - d)
-                forward(m, z - d)
-
-            @pl.when(z + d < nz)
-            def _():
-                arrived(m, z + d)
-                forward(m, z + d)
-    for d in range(1, nz - 1):
-        relay_wide(d)
-    own_unit(2)
+
+    def relay(m, d):
+        @pl.when(z - d >= 0)
+        def _():
+            arrived(m, z - d)
+            forward(m, z - d)
+
+        @pl.when(z + d < nz)
+        def _():
+            arrived(m, z + d)
+            forward(m, z + d)
+
+    side = z // (nz // 2)
+    edge = z + side * (nz - 1 - 2 * z)
+    late = (nz - 1) * (1 - side)
     inner = (z > 0) & (z < nz - 1)
 
-    def relay_down(d):
-        @pl.when(inner & (z - d >= 0))
-        def _():
-            arrived(2, z - d)
-            forward(2, z - d)
-
-        @pl.when(inner & (z + d < nz))
-        def _():
-            arrived(2, z + d)
-            forward(2, z + d)
-
-    end = z // (nz - 1)
-    late = (nz - 1) * (1 - end)
+    def normalize(k):
+        raw = tok.at[k] if k == 3 else psend.at[k]
+        block = rows // 6
+
+        @pl.loop(0, 6)
+        def _(i):
+            at = pl.ds(pl.multiple_of(i * block, 16), block)
+            values = raw[at, :].astype(jnp.float32)
+            scale = lax.rsqrt(jnp.mean(values * values, axis=-1, keepdims=True) + 1e-06)
+            tok[k, at, :] = (values * scale * gain_ref[...]).astype(jnp.bfloat16)
+
+    tiles = 2 * width // 256
+
+    def tile_at(i):
+        j = c * (tiles - 1) + i * (1 - 2 * c)
+        return pl.ds(pl.multiple_of(j * 256, 256), 256)
 
     def project(m, k, at, start, size):
         depths = pl.ds(pl.multiple_of(start * unit, 128), size * unit)
         return jnp.dot(tok[k, :, depths], gu[m, depths, at], preferred_element_type=jnp.float32)
 
+    def early(k):
+        @pl.loop(0, tiles)
+        def _(i):
+            at = tile_at(i)
+            for m in range(2):
+                acc[m, k, :, at] = project(m, k, at, side, nz - 1)
+
+    relay(0, 1)
+    relay(1, 1)
+    for h in range(2):
+        tok_part(1 + h, h).wait_recv()
+        tok_part(0, h).start()
+    for k in (1, 2, 0):
+        a2a(2, k).start()
+    local(2).start()
+    own_tok.wait()
+    normalize(3)
+    relay(0, 2)
+    for k in (1, 2):
+        tok_part(k, 2 - k).wait_recv()
+        normalize(k)
+    relay(1, 2)
     for m in range(2):
         for i in range(nz - 1):
-            from_sibling(m, end + i).wait_recv()
-    for k in (3, 1, 2, 0):
-        if k == 3:
-            own_tok.wait()
-        else:
-            tok_copy(k).wait_recv()
-        block = rows // 6
-
-        @pl.loop(0, 6)
+            from_sibling(m, side + i).wait_recv()
+    for k in (3, 1, 2):
+        early(k)
+    for h in range(2):
+        tok_part(0, h).wait_recv()
+    normalize(0)
+    early(0)
+    own_unit(2)
+
+    relay(0, nz - 1)
+    from_sibling(0, late).wait_recv()
+    for k in range(PLANE):
+        @pl.loop(0, tiles)
         def _(i):
-            at = pl.ds(pl.multiple_of(i * block, 16), block)
-            values = tok[k, at, :].astype(jnp.float32)
-            scale = lax.rsqrt(jnp.mean(values * values, axis=-1, keepdims=True) + 1e-06)
-            tok[k, at, :] = (values * scale * gain_ref[...]).astype(jnp.bfloat16)
-
-        @pl.loop(0, 2 * width // 256)
-        def _(j):
-            at = pl.ds(pl.multiple_of(j * 256, 256), 256)
-            for m in range(2):
-                acc[m, k, :, at] = project(m, k, at, end, nz - 1)
-
-    relay_wide(nz - 1)
-    for m in range(2):
-        from_sibling(m, late).wait_recv()
-
-    def make_hidden(k):
-        @pl.loop(0, 2 * width // 256)
-        def _(j):
-            at = pl.ds(pl.multiple_of(j * 256, 256), 256)
+            at = tile_at(i)
             gate = acc[0, k, :, at] + project(0, k, at, late, 1)
+            acc[0, k, :, at] = gate / (1.0 + jnp.exp(-gate))
+
+    for h in range(2):
+        tok_part(0, h).wait_send()
+    relay(1, nz - 1)
+
+    def make_hidden(k, start, stop):
+        @pl.loop(start, stop)
+        def _(i):
+            at = tile_at(i)
             up = acc[1, k, :, at] + project(1, k, at, late, 1)
-            hidden[k, :, at] = (gate / (1.0 + jnp.exp(-gate)) * up).astype(jnp.bfloat16)
-
-    part_rows = (pl.ds(0, rows // 2), pl.ds(rows // 2, rows // 2))
+            hidden[k, :, at] = (acc[0, k, :, at] * up).astype(jnp.bfloat16)
 
     def first(h, step):
         at = (0, part_rows[h], columns_at(step))
@@ -272,7 +297,9 @@
             device_id=dev(member(k), z, c), device_id_type=MESH)
 
     def plane_at(step):
-        return (z + step * (1 - 2 * (z // (nz // 2))) + nz) % nz
+        near = (2 * edge - step + nz) // nz
+        ahead = near * (1 - 2 * (step % 2)) * ((step + 1) // 2) + (1 - near) * (step - edge)
+        return z + ahead * (1 - 2 * side)
 
     def columns_at(step):
         return pl.ds(pl.multiple_of(plane_at(step) * unit, 128), unit)
@@ -295,11 +322,19 @@
                 arrived(2, zs)
                 to_sibling(2, zs).start()
 
-            relay_down(step)
+        if step % 2 == 1:
+            @pl.when(inner)
+            def _():
+                relay(2, (step + 1) // 2)
+
+        if step == 0:
+            for k in range(PLANE):
+                make_hidden(k, 0, tiles // 2)
+            from_sibling(1, late).wait_recv()
         from_sibling(2, zs).wait_recv()
         for k in range(PLANE):
             if step == 0:
-                make_hidden(k)
+                make_hidden(k, tiles // 2, tiles)
 
             @pl.loop(0, unit // 256)
             def _(j):
@@ -347,8 +382,9 @@
             @pl.when((zs >= z) & (z > 0))
             def _():
                 along(m, zs, -1).wait_send()
-    for k in range(3):
-        tok_copy(k).wait_send()
+    for k in (1, 2):
+        for h in range(2):
+            tok_part(k, h).wait_send()
     for step in range(nz):
         for h in range(2):
             first(h, step).wait_send()
@@ -379,7 +415,7 @@
             pltpu.VMEM((3, rows, features), bf16),
             pltpu.VMEM((3, rows, features), bf16),
             pltpu.VMEM((rows, features), jnp.float32),
-            dma((4,)), dma((3, 3)), dma((3, 3)), dma((3,)), dma((3,)),
+            dma((4,)), dma((3, 3)), dma((3, 3)), dma((3, 2)), dma((3, 2)),
             dma((3, nz)), dma((3, nz)), dma((3, nz)), dma((3, nz)), dma((3, nz)),
             dma((2, nz)), dma((2, nz)), dma((4, nz)), dma((4, nz)),
         ],
@@ -394,7 +430,7 @@
     fits = (
         ntp == 2
         and nfs % PLANE == 0
-        and (nfs // PLANE) % 2 == 0
+        and nfs == PLANE * PLANE
         and rows % 96 == 0
         and depth % 128 == 0
         and depth * nfs == tokens.shape[1]

time: 167 us -> 159 us (0.952)
  Pallas kernels: 164 us -> 156 us
    pallas_call x1, Pallas kernels: 164 us -> 156 us  [fused(): pl.pallas_call(functools.partial(kernel, nz), out_shape=jax.ShapeDtypeStr...]
where the time goes in v1:
time: 159 us; the launch traced here: 158 us
  Pallas kernels  156 us (98%)
  local copies, waits for them, and re-layouts  2.73 us (2%)
    pallas_call x1, Pallas kernels, fused(): pl.pallas_call(functools.partial(kernel, nz), out_shape=jax.ShapeDtypeStr...  156 us

profile of v1, /device:TPU:0, one launch (start us, length us, event | category | flops | bytes accessed | tf_op | source)
XLA Modules:
  0.0 158.4 jit_solution(1573305954302825039)
XLA Ops:
  0.0 155.6 %shard_map.55 = bf16[384,2048]{1,0:T(8,128)(2,1)} custom-call(bf16[768,2048]{1,0:T(8,128)(2,1)} %tok_hbm.1, f32[1,2048]{1,0:T(1,128)} %bitcast.1, bf16[128,2560]{1,0:T(8,128)(2,1)} %gate_hbm.1, bf16[128,2560]{1,0:T(8,128)(2,1)} %up_hbm.1, bf16[2560,128]{1,0:T(8,128)(2,1)} %down_hbm.1), custom_call_target="tpu_custom_call" | custom-call | tf_op jit(solution)/shard_map/pallas_call | solution.py:404
  155.6 2.7 %copy.7 = bf16[384,2048]{1,0:T(8,128)(2,1)} copy(bf16[384,2048]{1,0:T(8,128)(2,1)} %shard_map.55) | data formatting | bytes 3145728

commit v2 on v1

--- a/solution.py
+++ b/solution.py
@@ -33,7 +33,8 @@
 
 def kernel(nz, tok_hbm, gain_ref, gate_hbm, up_hbm, down_hbm, out_ref,
            tok, acc, gu, dn, hidden, psend, precv, own,
-           loc_sem, a2a_s, a2a_r, tok_s, tok_r, up_s, dn_s, z_r, sib_s, sib_r, one_s, one_r, rs_s, rs_r):
+           loc_sem, a2a_s, a2a_r, tok_s, tok_r, up_s, dn_s, z_r, sib_s, sib_r, end_s, end_r, pair_s, pair_r,
+           one_s, one_r, rs_s, rs_r):
     f = lax.axis_index("fs")
     c = lax.axis_index("tp")
     z, p = f // PLANE, f % PLANE
@@ -192,21 +193,66 @@
     own_unit(0)
     own_unit(1)
 
-    def relay(m, d):
-        @pl.when(z - d >= 0)
-        def _():
-            arrived(m, z - d)
-            forward(m, z - d)
-
-        @pl.when(z + d < nz)
-        def _():
-            arrived(m, z + d)
-            forward(m, z + d)
-
     side = z // (nz // 2)
     edge = z + side * (nz - 1 - 2 * z)
     late = (nz - 1) * (1 - side)
     inner = (z > 0) & (z < nz - 1)
+    outer = jnp.logical_not(inner)
+
+    def end_half(m, h):
+        ref = weight_dst(m, late * unit + h * (unit // 2), unit // 2)
+        return pltpu.make_async_remote_copy(
+            src_ref=ref, dst_ref=ref, send_sem=end_s.at[m - 1, h], recv_sem=end_r.at[m - 1, h],
+            device_id=dev(p, z + 2 * side - 1, c), device_id_type=MESH)
+
+    def pair_half(m, h, mine):
+        where = weight_dst if mine else weight_sib
+        ref = where(m, late * unit + h * (unit // 2), unit // 2)
+        return pltpu.make_async_remote_copy(
+            src_ref=ref, dst_ref=ref, send_sem=pair_s.at[m - 1, h], recv_sem=pair_r.at[m - 1, h],
+            device_id=(f, 1 - c), device_id_type=MESH)
+
+    def relay(m, d):
+        @pl.when(z - d >= 0)
+        def _():
+            arrived(m, z - d)
+            forward(m, z - d)
+
+        @pl.when(z + d < nz)
+        def _():
+            arrived(m, z + d)
+            forward(m, z + d)
+
+    def relay_far(m):
+        @pl.when(inner)
+        def _():
+            arrived(m, late)
+            for h in range(2):
+                end_half(m, h).start()
+            to_sibling(m, late).start()
+
+    def take(m, d):
+        @pl.when(outer)
+        def _():
+            zs = z + d * (1 - 2 * side)
+            arrived(m, zs)
+            to_sibling(m, zs).start()
+
+    def take_half(m, h):
+        @pl.when(outer)
+        def _():
+            end_half(m, h).wait_recv()
+            pair_half(m, h, True).start()
+
+    def paired_half(m, h):
+        @pl.when(outer)
+        def _():
+            pair_half(m, h, False).wait_recv()
+
+        if h == 0:
+            @pl.when(inner)
+            def _():
+                from_sibling(m, late).wait_recv()
 
     def normalize(k):
         raw = tok.at[k] if k == 3 else psend.at[k]
@@ -226,15 +272,18 @@
         return pl.ds(pl.multiple_of(j * 256, 256), 256)
 
     def project(m, k, at, start, size):
-        depths = pl.ds(pl.multiple_of(start * unit, 128), size * unit)
+        depths = pl.ds(pl.multiple_of(start, 128), size)
         return jnp.dot(tok[k, :, depths], gu[m, depths, at], preferred_element_type=jnp.float32)
 
-    def early(k):
+    def early(m, k):
         @pl.loop(0, tiles)
         def _(i):
             at = tile_at(i)
-            for m in range(2):
-                acc[m, k, :, at] = project(m, k, at, side, nz - 1)
+            acc[m, k, :, at] = project(m, k, at, side * unit, (nz - 1) * unit)
+
+    def all_paired(m):
+        for i in range(nz - 1):
+            from_sibling(m, side + i).wait_recv()
 
     relay(0, 1)
     relay(1, 1)
@@ -246,40 +295,51 @@
     local(2).start()
     own_tok.wait()
     normalize(3)
-    relay(0, 2)
+    relay(0, nz - 2)
+    all_paired(0)
+    early(0, 3)
     for k in (1, 2):
         tok_part(k, 2 - k).wait_recv()
         normalize(k)
-    relay(1, 2)
-    for m in range(2):
-        for i in range(nz - 1):
-            from_sibling(m, side + i).wait_recv()
+        early(0, k)
+    relay_far(1)
+    take(1, nz - 2)
+    all_paired(1)
     for k in (3, 1, 2):
-        early(k)
+        early(1, k)
     for h in range(2):
         tok_part(0, h).wait_recv()
     normalize(0)
-    early(0)
+    for m in range(2):
+        early(m, 0)
+
+    take(0, nz - 1)
     own_unit(2)
-
-    relay(0, nz - 1)
     from_sibling(0, late).wait_recv()
     for k in range(PLANE):
         @pl.loop(0, tiles)
         def _(i):
             at = tile_at(i)
-            gate = acc[0, k, :, at] + project(0, k, at, late, 1)
+            gate = acc[0, k, :, at] + project(0, k, at, late * unit, unit)
             acc[0, k, :, at] = gate / (1.0 + jnp.exp(-gate))
+
+    take_half(1, 0)
+    paired_half(1, 0)
+    for k in range(PLANE):
+        @pl.loop(0, tiles)
+        def _(i):
+            at = tile_at(i)
+            acc[1, k, :, at] += project(1, k, at, late * unit, unit // 2)
 
     for h in range(2):
         tok_part(0, h).wait_send()
-    relay(1, nz - 1)
+    take_half(1, 1)
 
     def make_hidden(k, start, stop):
         @pl.loop(start, stop)
         def _(i):
             at = tile_at(i)
-            up = acc[1, k, :, at] + project(1, k, at, late, 1)
+            up = acc[1, k, :, at] + project(1, k, at, late * unit + unit // 2, unit // 2)
             hidden[k, :, at] = (acc[0, k, :, at] * up).astype(jnp.bfloat16)
 
     def first(h, step):
@@ -301,8 +361,13 @@
         ahead = near * (1 - 2 * (step % 2)) * ((step + 1) // 2) + (1 - near) * (step - edge)
         return z + ahead * (1 - 2 * side)
 
-    def columns_at(step):
-        return pl.ds(pl.multiple_of(plane_at(step) * unit, 128), unit)
+    cuts = [(0, 0, 2), (0, 1, 2)] + [(step, 0, 1) for step in range(1, nz - 1)]
+    cuts += [(nz - 1, 0, 2), (nz - 1, 1, 2)]
+
+    def columns_at(i):
+        step, part, parts = cuts[i]
+        size = unit // parts
+        return pl.ds(pl.multiple_of(plane_at(step) * unit + part * size, 128), size)
 
     def add_and_send(step):
         for h in range(2):
@@ -314,31 +379,16 @@
             ).astype(jnp.bfloat16)
             last(k, h, step).start()
 
-    for step in range(nz):
-        zs = plane_at(step)
-        if step > 0:
-            @pl.when(jnp.logical_not(inner))
-            def _():
-                arrived(2, zs)
-                to_sibling(2, zs).start()
-
-        if step % 2 == 1:
-            @pl.when(inner)
-            def _():
-                relay(2, (step + 1) // 2)
-
-        if step == 0:
-            for k in range(PLANE):
-                make_hidden(k, 0, tiles // 2)
-            from_sibling(1, late).wait_recv()
-        from_sibling(2, zs).wait_recv()
+    def partials(i):
+        step, part, parts = cuts[i]
+        start, size = plane_at(step) * unit + part * (unit // parts), unit // parts
         for k in range(PLANE):
-            if step == 0:
+            if i == 0:
                 make_hidden(k, tiles // 2, tiles)
 
-            @pl.loop(0, unit // 256)
+            @pl.loop(0, size // 256)
             def _(j):
-                at = pl.ds(pl.multiple_of(zs * unit + j * 256, 256), 256)
+                at = pl.ds(pl.multiple_of(start + j * 256, 256), 256)
                 part = jnp.dot(hidden[k], dn[:, at], preferred_element_type=jnp.float32)
                 if k == 3:
                     own[:, at] = part
@@ -346,50 +396,84 @@
                     psend[k, :, at] = part.astype(jnp.bfloat16)
 
             if k == 0:
-                first(0, step).start()
-                first(1, step).start()
+                first(0, i).start()
+                first(1, i).start()
             elif k < 3:
-                last(k, k - 1, step).start()
+                last(k, k - 1, i).start()
+
+    for k in range(PLANE):
+        make_hidden(k, 0, tiles // 2)
+    paired_half(1, 1)
+    from_sibling(2, z).wait_recv()
+    final = len(cuts) - 1
+    for i in range(final + 1):
+        step, part, parts = cuts[i]
+        if i == final:
+            take_half(2, 1)
+            paired_half(2, 1)
+        elif i == final - 1:
+            take_half(2, 0)
+            paired_half(2, 0)
+        elif step > 0:
+            take(2, step)
+            from_sibling(2, plane_at(step)).wait_recv()
+        partials(i)
+        if i == 0:
+            continue
         if step == 0:
+            @pl.when(inner)
+            def _():
+                relay(2, 1)
+        elif step == nz - 2:
+            relay_far(2)
+        if i == 1:
             add_and_send(0)
-        elif step > 1:
-            add_and_send(step - 1)
-    add_and_send(nz - 1)
-
-    for step in range(nz):
+        add_and_send(i)
+
+    for i in range(final + 1):
+        at = columns_at(i)
         for k in (1, 2):
             for h in range(2):
-                last(k, h, step).wait_recv()
-
-        @pl.loop(0, unit // 256)
-        def _(j):
-            at = pl.ds(pl.multiple_of(plane_at(step) * unit + j * 256, 256), 256)
-            total = own[:, at]
-            for k in (1, 2):
-                total = total + precv[k, :, at].astype(jnp.float32)
-            out_ref[:, at] = total.astype(out_ref.dtype)
+                last(k, h, i).wait_recv()
+        total = own[:, at]
+        for k in (1, 2):
+            total = total + precv[k, :, at].astype(jnp.float32)
+        out_ref[:, at] = total.astype(out_ref.dtype)
 
     for m in range(3):
         for k in range(3):
             a2a(m, k).wait_send()
         for zs in range(nz):
-            to_sibling(m, zs).wait_send()
-
-            @pl.when((zs <= z) & (z < nz - 1))
+            whole = (zs - late) * (zs - late) > 0 if m > 0 else zs >= 0
+
+            @pl.when(inner | whole)
+            def _():
+                to_sibling(m, zs).wait_send()
+
+            @pl.when((zs <= z) & (z < nz - 1) & (outer | whole))
             def _():
                 along(m, zs, 1).wait_send()
 
-            @pl.when((zs >= z) & (z > 0))
+            @pl.when((zs >= z) & (z > 0) & (outer | whole))
             def _():
                 along(m, zs, -1).wait_send()
+    for m in (1, 2):
+        for h in range(2):
+            @pl.when(inner)
+            def _():
+                end_half(m, h).wait_send()
+
+            @pl.when(outer)
+            def _():
+                pair_half(m, h, True).wait_send()
     for k in (1, 2):
         for h in range(2):
             tok_part(k, h).wait_send()
-    for step in range(nz):
+    for i in range(final + 1):
         for h in range(2):
-            first(h, step).wait_send()
+            first(h, i).wait_send()
             for k in (1, 2):
-                last(k, h, step).wait_send()
+                last(k, h, i).wait_send()
 
 
 def fused(nfs, tokens, norm_gain, gate_weight, up_weight, down_weight):
@@ -403,7 +487,7 @@
     bf16 = jnp.bfloat16
     return pl.pallas_call(
         functools.partial(kernel, nz),
-        out_shape=jax.ShapeDtypeStruct((rows, features), bf16),
+        out_shape=pltpu.VMEM((rows, features), bf16),
         in_specs=[any_spec, vmem_spec, any_spec, any_spec, any_spec],
         out_specs=vmem_spec,
         scratch_shapes=[
@@ -417,10 +501,11 @@
             pltpu.VMEM((rows, features), jnp.float32),
             dma((4,)), dma((3, 3)), dma((3, 3)), dma((3, 2)), dma((3, 2)),
             dma((3, nz)), dma((3, nz)), dma((3, nz)), dma((3, nz)), dma((3, nz)),
-            dma((2, nz)), dma((2, nz)), dma((4, nz)), dma((4, nz)),
+            dma((2, 2)), dma((2, 2)), dma((2, 2)), dma((2, 2)),
+            dma((2, nz + 2)), dma((2, nz + 2)), dma((4, nz + 2)), dma((4, nz + 2)),
         ],
         compiler_params=pltpu.CompilerParams(
-            collective_id=0, has_side_effects=True, vmem_limit_bytes=62 * 1024 * 1024
+            collective_id=0, has_side_effects=True, vmem_limit_bytes=60 * 1024 * 1024
         ),
     )(tokens, norm_gain.reshape(1, features), gate_weight, up_weight, down_weight)
 

time: 159 us -> 153 us (0.962)
  Pallas kernels: 156 us -> 151 us
    pallas_call x1, Pallas kernels: 156 us -> 151 us  [fused(): pl.pallas_call(functools.partial(kernel, nz), out_shape=pltpu.VMEM((rows,...]
where the time goes in v2:
time: 153 us; the launch traced here: 152 us
  Pallas kernels  151 us (99%)
    pallas_call x1, Pallas kernels, fused(): pl.pallas_call(functools.partial(kernel, nz), out_shape=pltpu.VMEM((rows,...  151 us

profile of v2, /device:TPU:0, one launch (start us, length us, event | category | flops | bytes accessed | tf_op | source)
XLA Modules:
  0.0 152.5 jit_solution(15016252217366445059)
XLA Ops:
  0.0 151.3 %shard_map.55 = bf16[384,2048]{1,0:T(8,128)(2,1)S(1)} custom-call(bf16[768,2048]{1,0:T(8,128)(2,1)} %tok_hbm.1, f32[1,2048]{1,0:T(1,128)} %bitcast.1, bf16[128,2560]{1,0:T(8,128)(2,1)} %gate_hbm.1, bf16[128,2560]{1,0:T(8,128)(2,1)} %up_hbm.1, bf16[2560,128]{1,0:T(8,128)(2,1)} %down_hbm.1), custom_call_target="tpu_custom_call" | custom-call | tf_op jit(solution)/shard_map/pallas_call | solution.py:488
  151.3 1.1 copy.7

commit v3 on v2

--- a/solution.py
+++ b/solution.py
@@ -33,7 +33,7 @@
 
 def kernel(nz, tok_hbm, gain_ref, gate_hbm, up_hbm, down_hbm, out_ref,
            tok, acc, gu, dn, hidden, psend, precv, own,
-           loc_sem, a2a_s, a2a_r, tok_s, tok_r, up_s, dn_s, z_r, sib_s, sib_r, end_s, end_r, pair_s, pair_r,
+           loc_sem, a2a_s, a2a_r, tok_s, tok_r, up_s, dn_s, z_r, sib_s, sib_r, end_s, end_r, pair_s, pair_r, mid_s,
            one_s, one_r, rs_s, rs_r):
     f = lax.axis_index("fs")
     c = lax.axis_index("tp")
@@ -199,18 +199,49 @@
     inner = (z > 0) & (z < nz - 1)
     outer = jnp.logical_not(inner)
 
-    def end_half(m, h):
-        ref = weight_dst(m, late * unit + h * (unit // 2), unit // 2)
-        return pltpu.make_async_remote_copy(
-            src_ref=ref, dst_ref=ref, send_sem=end_s.at[m - 1, h], recv_sem=end_r.at[m - 1, h],
+    def end_half(m, zs, h):
+        ref = weight_dst(m, zs * unit + h * (unit // 2), unit // 2)
+        return pltpu.make_async_remote_copy(
+            src_ref=ref, dst_ref=ref, send_sem=end_s.at[m - 1, zs, h], recv_sem=end_r.at[m - 1, zs, h],
             device_id=dev(p, z + 2 * side - 1, c), device_id_type=MESH)
 
-    def pair_half(m, h, mine):
+    def pair_half(m, zs, h, mine):
         where = weight_dst if mine else weight_sib
-        ref = where(m, late * unit + h * (unit // 2), unit // 2)
-        return pltpu.make_async_remote_copy(
-            src_ref=ref, dst_ref=ref, send_sem=pair_s.at[m - 1, h], recv_sem=pair_r.at[m - 1, h],
+        ref = where(m, zs * unit + h * (unit // 2), unit // 2)
+        return pltpu.make_async_remote_copy(
+            src_ref=ref, dst_ref=ref, send_sem=pair_s.at[m - 1, zs, h], recv_sem=pair_r.at[m - 1, zs, h],
             device_id=(f, 1 - c), device_id_type=MESH)
+
+    def across(zs, start, size):
+        ref = weight_dst(2, start, size)
+        return pltpu.make_async_remote_copy(
+            src_ref=ref, dst_ref=ref, send_sem=mid_s.at[zs], recv_sem=z_r.at[2, zs],
+            device_id=dev(p, z + 1 - 2 * side, c), device_id_type=MESH)
+
+    def piece_out(q):
+        start = (z * PLANE + q) * depth
+        across(z, start, depth).start()
+        ref = weight_dst(2, start, depth)
+        half_at = 2 * q // PLANE
+        pltpu.make_async_remote_copy(
+            src_ref=ref, dst_ref=ref, send_sem=end_s.at[1, z, half_at], recv_sem=end_r.at[1, z, half_at],
+            device_id=dev(p, z + 2 * side - 1, c), device_id_type=MESH).start()
+
+    def own_down():
+        for k in (1, 2, 0):
+            a2a_in(2, k).wait_recv()
+        local(2).wait()
+        to_sibling(2, z).start()
+
+        @pl.when(outer)
+        def _():
+            for k in range(PLANE):
+                pass_piece(2, k)
+
+        @pl.when(inner)
+        def _():
+            for q in range(PLANE):
+                piece_out(q)
 
     def relay(m, d):
         @pl.when(z - d >= 0)
@@ -228,8 +259,21 @@
         def _():
             arrived(m, late)
             for h in range(2):
-                end_half(m, h).start()
+                end_half(m, late, h).start()
             to_sibling(m, late).start()
+
+    def relay_near():
+        @pl.when(inner)
+        def _():
+            zs = z + 1 - 2 * side
+            arrived(2, zs)
+            for h in range(2):
+                end_half(2, zs, h).start()
+            to_sibling(2, zs).start()
+            zs = z + 2 * side - 1
+            arrived(2, zs)
+            across(zs, zs * unit, unit).start()
+            to_sibling(2, zs).start()
 
     def take(m, d):
         @pl.when(outer)
@@ -238,21 +282,21 @@
             arrived(m, zs)
             to_sibling(m, zs).start()
 
-    def take_half(m, h):
+    def take_half(m, zs, h):
         @pl.when(outer)
         def _():
-            end_half(m, h).wait_recv()
-            pair_half(m, h, True).start()
-
-    def paired_half(m, h):
+            end_half(m, zs, h).wait_recv()
+            pair_half(m, zs, h, True).start()
+
+    def paired_half(m, zs, h):
         @pl.when(outer)
         def _():
-            pair_half(m, h, False).wait_recv()
+            pair_half(m, zs, h, False).wait_recv()
 
         if h == 0:
             @pl.when(inner)
             def _():
-                from_sibling(m, late).wait_recv()
+                from_sibling(m, zs).wait_recv()
 
     def normalize(k):
         raw = tok.at[k] if k == 3 else psend.at[k]
@@ -314,7 +358,7 @@
         early(m, 0)
 
     take(0, nz - 1)
-    own_unit(2)
+    own_down()
     from_sibling(0, late).wait_recv()
     for k in range(PLANE):
         @pl.loop(0, tiles)
@@ -323,8 +367,8 @@
             gate = acc[0, k, :, at] + project(0, k, at, late * unit, unit)
             acc[0, k, :, at] = gate / (1.0 + jnp.exp(-gate))
 
-    take_half(1, 0)
-    paired_half(1, 0)
+    take_half(1, late, 0)
+    paired_half(1, late, 0)
     for k in range(PLANE):
         @pl.loop(0, tiles)
         def _(i):
@@ -333,7 +377,7 @@
 
     for h in range(2):
         tok_part(0, h).wait_send()
-    take_half(1, 1)
+    take_half(1, late, 1)
 
     def make_hidden(k, start, stop):
         @pl.loop(start, stop)
@@ -361,13 +405,9 @@
         ahead = near * (1 - 2 * (step % 2)) * ((step + 1) // 2) + (1 - near) * (step - edge)
         return z + ahead * (1 - 2 * side)
 
-    cuts = [(0, 0, 2), (0, 1, 2)] + [(step, 0, 1) for step in range(1, nz - 1)]
-    cuts += [(nz - 1, 0, 2), (nz - 1, 1, 2)]
-
     def columns_at(i):
-        step, part, parts = cuts[i]
-        size = unit // parts
-        return pl.ds(pl.multiple_of(plane_at(step) * unit + part * size, 128), size)
+        size = unit // 2
+        return pl.ds(pl.multiple_of(plane_at(i // 2) * unit + i % 2 * size, 128), size)
 
     def add_and_send(step):
         for h in range(2):
@@ -380,55 +420,56 @@
             last(k, h, step).start()
 
     def partials(i):
-        step, part, parts = cuts[i]
-        start, size = plane_at(step) * unit + part * (unit // parts), unit // parts
-        for k in range(PLANE):
-            if i == 0:
-                make_hidden(k, tiles // 2, tiles)
-
-            @pl.loop(0, size // 256)
+        start = plane_at(i // 2) * unit + i % 2 * (unit // 2)
+
+        def down(low, high):
+            @pl.loop(0, unit // 512)
             def _(j):
                 at = pl.ds(pl.multiple_of(start + j * 256, 256), 256)
-                part = jnp.dot(hidden[k], dn[:, at], preferred_element_type=jnp.float32)
-                if k == 3:
-                    own[:, at] = part
-                else:
-                    psend[k, :, at] = part.astype(jnp.bfloat16)
-
-            if k == 0:
-                first(0, i).start()
-                first(1, i).start()
-            elif k < 3:
-                last(k, k - 1, i).start()
-
-    for k in range(PLANE):
+                left = hidden[low:high].reshape((high - low) * rows, 2 * width)
+                part = jnp.dot(left, dn[:, at], preferred_element_type=jnp.float32)
+                for k in range(low, high):
+                    block = part[(k - low) * rows:(k - low + 1) * rows]
+                    if k == 3:
+                        own[:, at] = block
+                    else:
+                        psend[k, :, at] = block.astype(jnp.bfloat16)
+
+        if i == 0:
+            make_hidden(0, tiles // 2, tiles)
+        down(0, 1)
+        first(0, i).start()
+        first(1, i).start()
+        if i == 0:
+            make_hidden(1, tiles // 2, tiles)
+            make_hidden(2, tiles // 2, tiles)
+            down(1, 3)
+        else:
+            down(1, 4)
+        last(1, 0, i).start()
+        last(2, 1, i).start()
+        if i == 0:
+            make_hidden(3, 0, tiles)
+            down(3, 4)
+
+    for k in range(3):
         make_hidden(k, 0, tiles // 2)
-    paired_half(1, 1)
+    paired_half(1, late, 1)
     from_sibling(2, z).wait_recv()
-    final = len(cuts) - 1
+    final = 2 * nz - 1
     for i in range(final + 1):
-        step, part, parts = cuts[i]
-        if i == final:
-            take_half(2, 1)
-            paired_half(2, 1)
-        elif i == final - 1:
-            take_half(2, 0)
-            paired_half(2, 0)
-        elif step > 0:
-            take(2, step)
-            from_sibling(2, plane_at(step)).wait_recv()
+        if i > 1:
+            paired_half(2, plane_at(i // 2), i % 2)
         partials(i)
-        if i == 0:
-            continue
-        if step == 0:
-            @pl.when(inner)
-            def _():
-                relay(2, 1)
-        elif step == nz - 2:
+        if i == 1:
+            relay_near()
+        if i == 4:
             relay_far(2)
-        if i == 1:
-            add_and_send(0)
-        add_and_send(i)
+        if i > 0:
+            add_and_send(i - 1)
+        if 0 < i < final:
+            take_half(2, plane_at((i + 1) // 2), (i + 1) % 2)
+    add_and_send(final)
 
     for i in range(final + 1):
         at = columns_at(i)
@@ -444,28 +485,36 @@
         for k in range(3):
             a2a(m, k).wait_send()
         for zs in range(nz):
-            whole = (zs - late) * (zs - late) > 0 if m > 0 else zs >= 0
+            whole = (zs >= 0, (zs - late) * (zs - late) > 0, zs == z)[m]
 
             @pl.when(inner | whole)
             def _():
                 to_sibling(m, zs).wait_send()
 
-            @pl.when((zs <= z) & (z < nz - 1) & (outer | whole))
+            @pl.when((zs <= z) & (z < nz - 1) & (outer | whole if m < 2 else outer))
             def _():
                 along(m, zs, 1).wait_send()
 
-            @pl.when((zs >= z) & (z > 0) & (outer | whole))
+            @pl.when((zs >= z) & (z > 0) & (outer | whole if m < 2 else outer))
             def _():
                 along(m, zs, -1).wait_send()
-    for m in (1, 2):
-        for h in range(2):
-            @pl.when(inner)
-            def _():
-                end_half(m, h).wait_send()
-
-            @pl.when(outer)
-            def _():
-                pair_half(m, h, True).wait_send()
+    for h in range(2):
+        @pl.when(inner)
+        def _():
+            end_half(1, late, h).wait_send()
+            for zs in (z, z + 1 - 2 * side, late):
+                end_half(2, zs, h).wait_send()
+
+        @pl.when(outer)
+        def _():
+            pair_half(1, late, h, True).wait_send()
+            for d in range(1, nz):
+                pair_half(2, z + d * (1 - 2 * side), h, True).wait_send()
+
+    @pl.when(inner)
+    def _():
+        for zs in (z, z + 2 * side - 1):
+            across(zs, zs * unit, unit).wait_send()
     for k in (1, 2):
         for h in range(2):
             tok_part(k, h).wait_send()
@@ -501,8 +550,8 @@
             pltpu.VMEM((rows, features), jnp.float32),
             dma((4,)), dma((3, 3)), dma((3, 3)), dma((3, 2)), dma((3, 2)),
             dma((3, nz)), dma((3, nz)), dma((3, nz)), dma((3, nz)), dma((3, nz)),
-            dma((2, 2)), dma((2, 2)), dma((2, 2)), dma((2, 2)),
-            dma((2, nz + 2)), dma((2, nz + 2)), dma((4, nz + 2)), dma((4, nz + 2)),
+            dma((2, nz, 2)), dma((2, nz, 2)), dma((2, nz, 2)), dma((2, nz, 2)), dma((nz,)),
+            dma((2, 2 * nz)), dma((2, 2 * nz)), dma((4, 2 * nz)), dma((4, 2 * nz)),
         ],
         compiler_params=pltpu.CompilerParams(
             collective_id=0, has_side_effects=True, vmem_limit_bytes=60 * 1024 * 1024

time: 153 us -> 151 us (0.987)
    pallas_call x1, Pallas kernels: 151 us -> 150 us  [fused(): pl.pallas_call(functools.partial(kernel, nz), out_shape=pltpu.VMEM((rows,...]
where the time goes in v3:
time: 151 us
  Pallas kernels  150 us (99%)
    pallas_call x1, Pallas kernels, fused(): pl.pallas_call(functools.partial(kernel, nz), out_shape=pltpu.VMEM((rows,...  150 us

profile of v3, /device:TPU:0, one launch (start us, length us, event | category | flops | bytes accessed | tf_op | source)
XLA Modules:
  0.0 150.8 jit_solution(7725580698551540577)
XLA Ops:
  0.0 149.6 %shard_map.55 = bf16[384,2048]{1,0:T(8,128)(2,1)S(1)} custom-call(bf16[768,2048]{1,0:T(8,128)(2,1)} %tok_hbm.1, f32[1,2048]{1,0:T(1,128)} %bitcast.1, bf16[128,2560]{1,0:T(8,128)(2,1)} %gate_hbm.1, bf16[128,2560]{1,0:T(8,128)(2,1)} %up_hbm.1, bf16[2560,128]{1,0:T(8,128)(2,1)} %down_hbm.1), custom_call_target="tpu_custom_call" | custom-call | tf_op jit(solution)/shard_map/pallas_call | solution.py:537
  149.6 1.1 copy.7

commit v4 on v3

--- a/solution.py
+++ b/solution.py
@@ -32,9 +32,9 @@
 
 
 def kernel(nz, tok_hbm, gain_ref, gate_hbm, up_hbm, down_hbm, out_ref,
-           tok, acc, gu, dn, hidden, psend, precv, own,
+           tok, acc, gu, dn, hidden, psend, precv, own, detour,
            loc_sem, a2a_s, a2a_r, tok_s, tok_r, up_s, dn_s, z_r, sib_s, sib_r, end_s, end_r, pair_s, pair_r, mid_s,
-           one_s, one_r, rs_s, rs_r):
+           one_s, one_r, rs_s, rs_r, det_s, det_r):
     f = lax.axis_index("fs")
     c = lax.axis_index("tp")
     z, p = f // PLANE, f % PLANE
@@ -340,51 +340,96 @@
     own_tok.wait()
     normalize(3)
     relay(0, nz - 2)
-    all_paired(0)
-    early(0, 3)
-    for k in (1, 2):
-        tok_part(k, 2 - k).wait_recv()
-        normalize(k)
-        early(0, k)
-    relay_far(1)
-    take(1, nz - 2)
-    all_paired(1)
-    for k in (3, 1, 2):
-        early(1, k)
-    for h in range(2):
-        tok_part(0, h).wait_recv()
-    normalize(0)
-    for m in range(2):
-        early(m, 0)
-
-    take(0, nz - 1)
-    own_down()
-    from_sibling(0, late).wait_recv()
-    for k in range(PLANE):
+
+    def gated(k, start, size, add):
         @pl.loop(0, tiles)
         def _(i):
             at = tile_at(i)
-            gate = acc[0, k, :, at] + project(0, k, at, late * unit, unit)
+            gate = project(0, k, at, start, size)
+            if add:
+                gate = acc[0, k, :, at] + gate
             acc[0, k, :, at] = gate / (1.0 + jnp.exp(-gate))
 
-    take_half(1, late, 0)
-    paired_half(1, late, 0)
-    for k in range(PLANE):
-        @pl.loop(0, tiles)
-        def _(i):
-            at = tile_at(i)
-            acc[1, k, :, at] += project(1, k, at, late * unit, unit // 2)
-
-    for h in range(2):
-        tok_part(0, h).wait_send()
-    take_half(1, late, 1)
-
-    def make_hidden(k, start, stop):
-        @pl.loop(start, stop)
+    def make_hidden(k, low, high):
+        @pl.loop(low, high)
         def _(i):
             at = tile_at(i)
             up = acc[1, k, :, at] + project(1, k, at, late * unit + unit // 2, unit // 2)
             hidden[k, :, at] = (acc[0, k, :, at] * up).astype(jnp.bfloat16)
+
+    def neighbours_tokens():
+        for k in (1, 2):
+            tok_part(k, 2 - k).wait_recv()
+            normalize(k)
+
+    def diagonal_tokens():
+        for h in range(2):
+            tok_part(0, h).wait_recv()
+        normalize(0)
+
+    @pl.when(inner)
+    def _():
+        all_paired(0)
+        from_sibling(0, late).wait_recv()
+
+        def whole_hidden(k):
+            @pl.loop(0, tiles)
+            def _(i):
+                at = tile_at(i)
+                up = project(1, k, at, 0, nz * unit)
+                hidden[k, :, at] = (acc[0, k, :, at] * up).astype(jnp.bfloat16)
+
+        gated(3, 0, nz * unit, False)
+        neighbours_tokens()
+        gated(1, 0, nz * unit, False)
+        relay_far(1)
+        gated(2, 0, nz * unit, False)
+        all_paired(1)
+        from_sibling(1, late).wait_recv()
+        for k in (1, 2):
+            whole_hidden(k)
+        diagonal_tokens()
+        gated(0, 0, nz * unit, False)
+        own_down()
+        whole_hidden(0)
+
+    @pl.when(outer)
+    def _():
+        all_paired(0)
+        early(0, 3)
+        for k in (1, 2):
+            tok_part(k, 2 - k).wait_recv()
+            normalize(k)
+            early(0, k)
+        take(1, nz - 2)
+        all_paired(1)
+        for k in (3, 1, 2):
+            early(1, k)
+        diagonal_tokens()
+        for m in range(2):
+            early(m, 0)
+
+        take(0, nz - 1)
+        own_down()
+        from_sibling(0, late).wait_recv()
+        for k in range(PLANE):
+            gated(k, late * unit, unit, True)
+        take_half(1, late, 0)
+        pair_half(1, late, 0, False).wait_recv()
+        for k in range(PLANE):
+            @pl.loop(0, tiles)
+            def _(i):
+                at = tile_at(i)
+                acc[1, k, :, at] += project(1, k, at, late * unit, unit // 2)
+
+        take_half(1, late, 1)
+        for k in range(3):
+            make_hidden(k, 0, tiles // 2)
+        pair_half(1, late, 1, False).wait_recv()
+        make_hidden(0, tiles // 2, tiles)
+
+    for h in range(2):
+        tok_part(0, h).wait_send()
 
     def first(h, step):
         at = (0, part_rows[h], columns_at(step))
@@ -435,26 +480,65 @@
                     else:
                         psend[k, :, at] = block.astype(jnp.bfloat16)
 
-        if i == 0:
-            make_hidden(0, tiles // 2, tiles)
         down(0, 1)
         first(0, i).start()
         first(1, i).start()
         if i == 0:
-            make_hidden(1, tiles // 2, tiles)
-            make_hidden(2, tiles // 2, tiles)
+            @pl.when(outer)
+            def _():
+                make_hidden(1, tiles // 2, tiles)
+                make_hidden(2, tiles // 2, tiles)
+
             down(1, 3)
         else:
             down(1, 4)
-        last(1, 0, i).start()
-        last(2, 1, i).start()
+        if i < 2:
+            @pl.when(outer)
+            def _():
+                for k in (1, 2):
+                    leave(k, i).start()
+
+            @pl.when(inner)
+            def _():
+                last(1, 0, i).start()
+                last(2, 1, i).start()
+        else:
+            last(1, 0, i).start()
+            last(2, 1, i).start()
         if i == 0:
-            make_hidden(3, 0, tiles)
+            @pl.when(outer)
+            def _():
+                make_hidden(3, 0, tiles)
+
+            @pl.when(inner)
+            def _():
+                @pl.loop(0, tiles)
+                def _(i):
+                    at = tile_at(i)
+                    up = project(1, 3, at, 0, nz * unit)
+                    hidden[3, :, at] = (acc[0, 3, :, at] * up).astype(jnp.bfloat16)
+
             down(3, 4)
 
-    for k in range(3):
-        make_hidden(k, 0, tiles // 2)
-    paired_half(1, late, 1)
+    def stage(number, k, i, to, src, dst, arrival):
+        return pltpu.make_async_remote_copy(
+            src_ref=src, dst_ref=dst, send_sem=det_s.at[number, k - 1, i], recv_sem=arrival,
+            device_id=to, device_id_type=MESH)
+
+    def leave(k, i):
+        return stage(0, k, i, dev(p, z + 1 - 2 * side, c), psend.at[k, part_rows[k - 1], columns_at(i)],
+                     detour.at[0, k - 1, i], det_r.at[0, k - 1, i])
+
+    def cross(k, i):
+        return stage(1, k, i, dev(member(k), z, c), detour.at[0, k - 1, i],
+                     detour.at[1, k - 1, i], det_r.at[1, k - 1, i])
+
+    def come_back(k, i):
+        zs = z + 2 * side - 1
+        start = pl.multiple_of(zs * unit + i * (unit // 2), 128)
+        return stage(2, k, i, dev(p, zs, c), detour.at[1, k - 1, i],
+                     precv.at[k, part_rows[k - 1], pl.ds(start, unit // 2)], rs_r.at[3 * k - 3, i])
+
     from_sibling(2, z).wait_recv()
     final = 2 * nz - 1
     for i in range(final + 1):
@@ -462,11 +546,34 @@
             paired_half(2, plane_at(i // 2), i % 2)
         partials(i)
         if i == 1:
+            add_and_send(0)
             relay_near()
+
+            @pl.when(inner)
+            def _():
+                add_and_send(1)
+        elif i == 2:
+            @pl.when(outer)
+            def _():
+                add_and_send(1)
+        elif i > 2:
+            add_and_send(i - 1)
         if i == 4:
+            @pl.when(inner)
+            def _():
+                for j in range(2):
+                    for k in (1, 2):
+                        leave(k, j).wait_recv()
+                        cross(k, j).start()
+        if i == 5:
             relay_far(2)
-        if i > 0:
-            add_and_send(i - 1)
+        if i == 7:
+            @pl.when(inner)
+            def _():
+                for j in range(2):
+                    for k in (1, 2):
+                        cross(k, j).wait_recv()
+                        come_back(k, j).start()
         if 0 < i < final:
             take_half(2, plane_at((i + 1) // 2), (i + 1) % 2)
     add_and_send(final)
@@ -522,7 +629,18 @@
         for h in range(2):
             first(h, i).wait_send()
             for k in (1, 2):
-                last(k, h, i).wait_send()
+                if i < 2 and h == k - 1:
+                    @pl.when(inner)
+                    def _():
+                        last(k, h, i).wait_send()
+                        cross(k, i).wait_send()
+                        come_back(k, i).wait_send()
+
+                    @pl.when(outer)
+                    def _():
+                        leave(k, i).wait_send()
+                else:
+                    last(k, h, i).wait_send()
 
 
 def fused(nfs, tokens, norm_gain, gate_weight, up_weight, down_weight):
@@ -548,10 +666,12 @@
             pltpu.VMEM((3, rows, features), bf16),
             pltpu.VMEM((3, rows, features), bf16),
             pltpu.VMEM((rows, features), jnp.float32),
+            pltpu.VMEM((2, 2, 2, rows // 2, features // (2 * nz)), bf16),
             dma((4,)), dma((3, 3)), dma((3, 3)), dma((3, 2)), dma((3, 2)),
             dma((3, nz)), dma((3, nz)), dma((3, nz)), dma((3, nz)), dma((3, nz)),
             dma((2, nz, 2)), dma((2, nz, 2)), dma((2, nz, 2)), dma((2, nz, 2)), dma((nz,)),
             dma((2, 2 * nz)), dma((2, 2 * nz)), dma((4, 2 * nz)), dma((4, 2 * nz)),
+            dma((3, 2, 2)), dma((2, 2, 2)),
         ],
         compiler_params=pltpu.CompilerParams(
             collective_id=0, has_side_effects=True, vmem_limit_bytes=60 * 1024 * 1024

time: 151 us -> 149 us (0.987)
  Pallas kernels: 150 us -> 148 us
    pallas_call x1, Pallas kernels: 150 us -> 148 us  [fused(): pl.pallas_call(functools.partial(kernel, nz), out_shape=pltpu.VMEM((rows,...]
where the time goes in v4:
time: 149 us
  Pallas kernels  148 us (99%)
    pallas_call x1, Pallas kernels, fused(): pl.pallas_call(functools.partial(kernel, nz), out_shape=pltpu.VMEM((rows,...  148 us

profile of v4, /device:TPU:0, one launch (start us, length us, event | category | flops | bytes accessed | tf_op | source)
XLA Modules:
  0.0 149.1 jit_solution(2244814336792045935)
XLA Ops:
  0.0 148.0 %shard_map.55 = bf16[384,2048]{1,0:T(8,128)(2,1)S(1)} custom-call(bf16[768,2048]{1,0:T(8,128)(2,1)} %tok_hbm.1, f32[1,2048]{1,0:T(1,128)} %bitcast.1, bf16[128,2560]{1,0:T(8,128)(2,1)} %gate_hbm.1, bf16[128,2560]{1,0:T(8,128)(2,1)} %up_hbm.1, bf16[2560,128]{1,0:T(8,128)(2,1)} %down_hbm.1), custom_call_target="tpu_custom_call" | custom-call | tf_op jit(solution)/shard_map/pallas_call | solution.py:655
  148.0 1.1 copy.7

commit v5 on v4

--- a/solution.py
+++ b/solution.py
@@ -31,8 +31,8 @@
     )
 
 
-def kernel(nz, tok_hbm, gain_ref, gate_hbm, up_hbm, down_hbm, out_ref,
-           tok, acc, gu, dn, hidden, psend, precv, own, detour,
+def kernel(nz, tok_hbm, gain_hbm, gate_hbm, up_hbm, down_hbm, out_ref,
+           gain_ref, tok, acc, gu, dn, hidden, psend, precv, own, detour,
            loc_sem, a2a_s, a2a_r, tok_s, tok_r, up_s, dn_s, z_r, sib_s, sib_r, end_s, end_r, pair_s, pair_r, mid_s,
            one_s, one_r, rs_s, rs_r, det_s, det_r):
     f = lax.axis_index("fs")
@@ -180,6 +180,8 @@
         tok_part(1, h).start()
         tok_part(2, 1 - h).start()
     own_tok.start()
+    gain = pltpu.make_async_copy(gain_hbm, gain_ref, loc_sem.at[4])
+    gain.start()
 
     def own_unit(m):
         if m == 2:
@@ -199,15 +201,22 @@
     inner = (z > 0) & (z < nz - 1)
     outer = jnp.logical_not(inner)
 
-    def end_half(m, zs, h):
-        ref = weight_dst(m, zs * unit + h * (unit // 2), unit // 2)
+    def split(h, parts):
+        if parts == 2 or h == 0:
+            return h * (unit // 2), unit // 2
+        return (h + 1) * (unit // 4), unit // 4
+
+    def end_part(m, zs, h, parts):
+        start, size = split(h, parts)
+        ref = weight_dst(m, zs * unit + start, size)
         return pltpu.make_async_remote_copy(
             src_ref=ref, dst_ref=ref, send_sem=end_s.at[m - 1, zs, h], recv_sem=end_r.at[m - 1, zs, h],
             device_id=dev(p, z + 2 * side - 1, c), device_id_type=MESH)
 
-    def pair_half(m, zs, h, mine):
+    def pair_part(m, zs, h, parts, mine):
         where = weight_dst if mine else weight_sib
-        ref = where(m, zs * unit + h * (unit // 2), unit // 2)
+        start, size = split(h, parts)
+        ref = where(m, zs * unit + start, size)
         return pltpu.make_async_remote_copy(
             src_ref=ref, dst_ref=ref, send_sem=pair_s.at[m - 1, zs, h], recv_sem=pair_r.at[m - 1, zs, h],
             device_id=(f, 1 - c), device_id_type=MESH)
@@ -258,8 +267,8 @@
         @pl.when(inner)
         def _():
             arrived(m, late)
-            for h in range(2):
-                end_half(m, late, h).start()
+            for h in range(m + 1):
+                end_part(m, late, h, m + 1).start()
             to_sibling(m, late).start()
 
     def relay_near():
@@ -268,7 +277,7 @@
             zs = z + 1 - 2 * side
             arrived(2, zs)
             for h in range(2):
-                end_half(2, zs, h).start()
+                end_part(2, zs, h, 2).start()
             to_sibling(2, zs).start()
             zs = z + 2 * side - 1
             arrived(2, zs)
@@ -282,16 +291,16 @@
             arrived(m, zs)
             to_sibling(m, zs).start()
 
-    def take_half(m, zs, h):
+    def take_part(m, zs, h, parts):
         @pl.when(outer)
         def _():
-            end_half(m, zs, h).wait_recv()
-            pair_half(m, zs, h, True).start()
-
-    def paired_half(m, zs, h):
+            end_part(m, zs, h, parts).wait_recv()
+            pair_part(m, zs, h, parts, True).start()
+
+    def paired_part(m, zs, h, parts):
         @pl.when(outer)
         def _():
-            pair_half(m, zs, h, False).wait_recv()
+            pair_part(m, zs, h, parts, False).wait_recv()
 
         if h == 0:
             @pl.when(inner)
@@ -338,6 +347,7 @@
         a2a(2, k).start()
     local(2).start()
     own_tok.wait()
+    gain.wait()
     normalize(3)
     relay(0, nz - 2)
 
@@ -414,18 +424,18 @@
         from_sibling(0, late).wait_recv()
         for k in range(PLANE):
             gated(k, late * unit, unit, True)
-        take_half(1, late, 0)
-        pair_half(1, late, 0, False).wait_recv()
+        take_part(1, late, 0, 2)
+        pair_part(1, late, 0, 2, False).wait_recv()
         for k in range(PLANE):
             @pl.loop(0, tiles)
             def _(i):
                 at = tile_at(i)
                 acc[1, k, :, at] += project(1, k, at, late * unit, unit // 2)
 
-        take_half(1, late, 1)
+        take_part(1, late, 1, 2)
         for k in range(3):
             make_hidden(k, 0, tiles // 2)
-        pair_half(1, late, 1, False).wait_recv()
+        pair_part(1, late, 1, 2, False).wait_recv()
         make_hidden(0, tiles // 2, tiles)
 
     for h in range(2):
@@ -450,9 +460,13 @@
         ahead = near * (1 - 2 * (step % 2)) * ((step + 1) // 2) + (1 - near) * (step - edge)
         return z + ahead * (1 - 2 * side)
 
+    final = 2 * nz
+    cuts = [(step, h, 2) for step in range(nz - 1) for h in range(2)] + [(nz - 1, h, 3) for h in range(3)]
+
     def columns_at(i):
-        size = unit // 2
-        return pl.ds(pl.multiple_of(plane_at(i // 2) * unit + i % 2 * size, 128), size)
+        step, h, parts = cuts[i]
+        start, size = split(h, parts)
+        return pl.ds(pl.multiple_of(plane_at(step) * unit + start, 128), size)
 
     def add_and_send(step):
         for h in range(2):
@@ -465,12 +479,14 @@
             last(k, h, step).start()
 
     def partials(i):
-        start = plane_at(i // 2) * unit + i % 2 * (unit // 2)
+        step, h, parts = cuts[i]
+        start, size = split(h, parts)
+        start, tile = plane_at(step) * unit + start, 128 if size % 256 else 256
 
         def down(low, high):
-            @pl.loop(0, unit // 512)
+            @pl.loop(0, size // tile)
             def _(j):
-                at = pl.ds(pl.multiple_of(start + j * 256, 256), 256)
+                at = pl.ds(pl.multiple_of(start + j * tile, 128), tile)
                 left = hidden[low:high].reshape((high - low) * rows, 2 * width)
                 part = jnp.dot(left, dn[:, at], preferred_element_type=jnp.float32)
                 for k in range(low, high):
@@ -483,6 +499,9 @@
         down(0, 1)
         first(0, i).start()
         first(1, i).start()
+        if i == final:
+            last(1, 0, i - 1).start()
+            last(2, 1, i - 1).start()
         if i == 0:
             @pl.when(outer)
             def _():
@@ -502,7 +521,7 @@
             def _():
                 last(1, 0, i).start()
                 last(2, 1, i).start()
-        else:
+        elif i != final - 1:
             last(1, 0, i).start()
             last(2, 1, i).start()
         if i == 0:
@@ -540,10 +559,9 @@
                      precv.at[k, part_rows[k - 1], pl.ds(start, unit // 2)], rs_r.at[3 * k - 3, i])
 
     from_sibling(2, z).wait_recv()
-    final = 2 * nz - 1
     for i in range(final + 1):
         if i > 1:
-            paired_half(2, plane_at(i // 2), i % 2)
+            paired_part(2, plane_at(cuts[i][0]), *cuts[i][1:])
         partials(i)
         if i == 1:
             add_and_send(0)
@@ -575,7 +593,7 @@
                         cross(k, j).wait_recv()
                         come_back(k, j).start()
         if 0 < i < final:
-            take_half(2, plane_at((i + 1) // 2), (i + 1) % 2)
+            take_part(2, plane_at(cuts[i + 1][0]), *cuts[i + 1][1:])
     add_and_send(final)
 
     for i in range(final + 1):
@@ -605,18 +623,17 @@
             @pl.when((zs >= z) & (z > 0) & (outer | whole if m < 2 else outer))
             def _():
                 along(m, zs, -1).wait_send()
-    for h in range(2):
+    pieces = [(1, nz - 1, h, 2) for h in range(2)] + [(2, nz - 1, h, 3) for h in range(3)]
+    pieces += [(2, d, h, 2) for d in range(1, nz - 1) for h in range(2)]
+    for m, d, h, parts in pieces:
         @pl.when(inner)
         def _():
-            end_half(1, late, h).wait_send()
-            for zs in (z, z + 1 - 2 * side, late):
-                end_half(2, zs, h).wait_send()
+            zs = late if d == nz - 1 else z + (d - 1) * (1 - 2 * side)
+            end_part(m, zs, h, parts).wait_send()
 
         @pl.when(outer)
         def _():
-            pair_half(1, late, h, True).wait_send()
-            for d in range(1, nz):
-                pair_half(2, z + d * (1 - 2 * side), h, True).wait_send()
+            pair_part(m, z + d * (1 - 2 * side), h, parts, True).wait_send()
 
     @pl.when(inner)
     def _():
@@ -655,9 +672,10 @@
     return pl.pallas_call(
         functools.partial(kernel, nz),
         out_shape=pltpu.VMEM((rows, features), bf16),
-        in_specs=[any_spec, vmem_spec, any_spec, any_spec, any_spec],
+        in_specs=[any_spec] * 5,
         out_specs=vmem_spec,
         scratch_shapes=[
+            pltpu.VMEM((1, features), jnp.float32),
             pltpu.VMEM((PLANE, rows, features), bf16),
             pltpu.VMEM((2, PLANE, rows, 2 * width), jnp.float32),
             pltpu.VMEM((2, features, 2 * width), bf16),
@@ -667,10 +685,10 @@
             pltpu.VMEM((3, rows, features), bf16),
             pltpu.VMEM((rows, features), jnp.float32),
             pltpu.VMEM((2, 2, 2, rows // 2, features // (2 * nz)), bf16),
-            dma((4,)), dma((3, 3)), dma((3, 3)), dma((3, 2)), dma((3, 2)),
+            dma((5,)), dma((3, 3)), dma((3, 3)), dma((3, 2)), dma((3, 2)),
             dma((3, nz)), dma((3, nz)), dma((3, nz)), dma((3, nz)), dma((3, nz)),
-            dma((2, nz, 2)), dma((2, nz, 2)), dma((2, nz, 2)), dma((2, nz, 2)), dma((nz,)),
-            dma((2, 2 * nz)), dma((2, 2 * nz)), dma((4, 2 * nz)), dma((4, 2 * nz)),
+            dma((2, nz, 3)), dma((2, nz, 3)), dma((2, nz, 3)), dma((2, nz, 3)), dma((nz,)),
+            dma((2, 2 * nz + 1)), dma((2, 2 * nz + 1)), dma((4, 2 * nz + 1)), dma((4, 2 * nz + 1)),
             dma((3, 2, 2)), dma((2, 2, 2)),
         ],
         compiler_params=pltpu.CompilerParams(

time: 149 us -> 148 us (level)
  no operation moved by 1% of the time
where the time goes in v5:
time: 148 us
  Pallas kernels  147 us (99%)
    pallas_call x1, Pallas kernels, fused(): pl.pallas_call(functools.partial(kernel, nz), out_shape=pltpu.VMEM((rows,...  147 us

profile of v5, /device:TPU:0, one launch (start us, length us, event | category | flops | bytes accessed | tf_op | source)
XLA Modules:
  0.0 148.1 jit_solution(8336848239464304900)
XLA Ops:
  0.0 147.0 %shard_map.55 = bf16[384,2048]{1,0:T(8,128)(2,1)S(1)} custom-call(bf16[768,2048]{1,0:T(8,128)(2,1)} %tok_hbm.1, f32[1,2048]{1,0:T(1,128)} %bitcast.1, bf16[128,2560]{1,0:T(8,128)(2,1)} %gate_hbm.1, bf16[128,2560]{1,0:T(8,128)(2,1)} %up_hbm.1, bf16[2560,128]{1,0:T(8,128)(2,1)} %down_hbm.1), custom_call_target="tpu_custom_call" | custom-call | tf_op jit(solution)/shard_map/pallas_call | solution.py:672
  147.0 1.1 copy.7
